TPU v7x, 32 devices: a whole 2x2x4 slice. The times are simulated.
32 devices in a mesh: kv: 16 (over z, y, x), tp: 2 (over core).
Axes of the slice: x: 2, y: 2, z: 4, core: 2. Of those that a mesh axis runs over, the one named last changes fastest.
Arguments:
- tokens: bfloat16 [4096, 2048], P('kv'), may hold values from -40 to 40
- query_weight: bfloat16 [2048, 2048], P(None, 'tp'), may hold values from -0.125 to 0.125
- key_matrix: bfloat16 [2048, 1024], P(None, 'tp'), may hold values from -0.125 to 0.125
- value_matrix: bfloat16 [2048, 1024], P(None, 'tp'), may hold values from -0.125 to 0.125
- gate_weight: bfloat16 [2, 2048, 16], replicated, may hold values from -0.125 to 0.125
- key_pool_weight: float32 [16, 8], replicated, may hold values from -1.5 to 1.5
- value_pool_weight: float32 [16, 8], replicated, may hold values from -1.5 to 1.5
- out_weight: bfloat16 [2048, 2048], P('tp'), may hold values from -0.125 to 0.125
- chosen: int32 [64, 32], P('kv'), may hold values from 0 to 63, as said below
Outputs:
- mixed: bfloat16 [4096, 2048], P(('kv', 'tp'))
- log_sums: float32 [4096, 16], P('kv', 'tp')
Inputs may be any that keep to these rules, and one draw needn't show every extreme that they name: `chosen`: row i names only blocks <= i and names block i in its first column; a block may stand several times in a row and counts each time. The rows of one index of kv name, together, at most 2 distinct blocks held by any one other index, and exactly 2 of the index just before it whenever there is one.
All inputs are finite; a program needn't handle non-finite values.
Results may differ from a plain program's by a relative error of at most 0.018.
Values may be sent and summed in bfloat16 or wider, within the bound.
A program may use at most 128 MiB of HBM per device.

v0:
```python
import jax
import jax.numpy as jnp
from jax import lax
from jax.sharding import PartitionSpec as P

HEAD_SIZE = 128
BLOCK_LENGTH = 64
POOL_STRIDE = 16
PICKED_BLOCKS = 32
CAP = 2


THETA = 10000.0
NEGATIVE = -1e30


def apply_rotary(values_in, positions):
    half_width = values_in.shape[-1] // 2
    inverse = THETA ** (-jnp.arange(half_width, dtype=jnp.float32) / half_width)
    angles = positions.astype(jnp.float32)[:, None] * inverse[None, :]
    cosines = jnp.cos(angles)[:, None, :]
    sines = jnp.sin(angles)[:, None, :]
    front_half = values_in[..., :half_width]
    back_half = values_in[..., half_width:]
    return jnp.concatenate(
        [front_half * cosines - back_half * sines, back_half * cosines + front_half * sines],
        axis=-1,
    )


def shards(
    tokens,
    query_weight,
    key_matrix,
    value_matrix,
    gate_weight,
    key_pool_weight,
    value_pool_weight,
    out_weight,
    chosen,
):
    row_count = tokens.shape[0]
    kv_size = lax.axis_size("kv")
    own_index = lax.axis_index("kv")
    head_count = query_weight.shape[1] // HEAD_SIZE
    kv_heads = key_matrix.shape[1] // HEAD_SIZE
    group_count_heads = head_count // kv_heads
    start_point = own_index * row_count
    positions = start_point + jnp.arange(row_count, dtype=jnp.int32)
    query_proj = jnp.dot(tokens, query_weight, preferred_element_type=jnp.float32).reshape(
        row_count, head_count, HEAD_SIZE
    )
    key_projected = jnp.dot(tokens, key_matrix, preferred_element_type=jnp.float32).reshape(
        row_count, kv_heads, HEAD_SIZE
    )
    value_projected = jnp.dot(tokens, value_matrix, preferred_element_type=jnp.float32).reshape(
        row_count, kv_heads, HEAD_SIZE
    )
    query_states = apply_rotary(query_proj, positions).astype(jnp.bfloat16)
    key_states = apply_rotary(key_projected, positions).astype(jnp.bfloat16)
    value_states = value_projected.astype(jnp.bfloat16)
    head_start = lax.axis_index("tp") * head_count
    kv_start = lax.axis_index("tp") * kv_heads
    key_mix = lax.dynamic_slice_in_dim(key_pool_weight, kv_start, kv_heads, 1)
    value_mix = lax.dynamic_slice_in_dim(value_pool_weight, kv_start, kv_heads, 1)
    pooled_here = row_count // POOL_STRIDE
    block_ends = (
        start_point + POOL_STRIDE * jnp.arange(pooled_here, dtype=jnp.int32) + POOL_STRIDE - 1
    )
    compact_keys = apply_rotary(
        jnp.einsum(
            "cwyi,wy->cyi",
            key_projected.reshape(pooled_here, POOL_STRIDE, kv_heads, HEAD_SIZE),
            key_mix,
            precision=lax.Precision.HIGHEST,
        ),
        block_ends,
    ).astype(jnp.bfloat16)
    compact_values = jnp.einsum(
        "cwyi,wy->cyi",
        value_projected.reshape(pooled_here, POOL_STRIDE, kv_heads, HEAD_SIZE),
        value_mix,
        precision=lax.Precision.HIGHEST,
    ).astype(jnp.bfloat16)
    all_keys, all_values = (
        lax.all_gather(compact_keys, "kv", axis=0, tiled=True),
        lax.all_gather(compact_values, "kv", axis=0, tiled=True),
    )
    gate_cols = lax.dynamic_slice_in_dim(gate_weight, head_start, head_count, 2)
    gate_values = jax.nn.sigmoid(
        jnp.einsum("td,bdh->bth", tokens, gate_cols, preferred_element_type=jnp.float32)
    )
    score_scale = HEAD_SIZE ** (-0.5)
    grouped = query_states.reshape(row_count, kv_heads, group_count_heads, HEAD_SIZE)
    pooled_total = all_keys.shape[0]
    pooled_ends = POOL_STRIDE * jnp.arange(pooled_total, dtype=jnp.int32) + POOL_STRIDE - 1
    visible = (pooled_ends[None, :] <= positions[:, None]) | (
        jnp.arange(pooled_total)[None, :] == 0
    )
    scores = (
        jnp.einsum("qgjd,ngd->gjqn", grouped, all_keys, preferred_element_type=jnp.float32)
        * score_scale
    )
    masked = jnp.where(visible, scores, NEGATIVE)
    peak_value = jnp.max(masked, axis=-1, keepdims=True)
    exponent = jnp.where(visible, jnp.exp(masked - peak_value), 0.0)
    weights = (exponent / jnp.sum(exponent, axis=-1, keepdims=True)).astype(jnp.bfloat16)
    pooled_out = jnp.einsum(
        "gjqn,ngd->qgjd", weights, all_values, preferred_element_type=jnp.float32
    )
    row_width = kv_heads * 2 * HEAD_SIZE
    kv_rows = jnp.concatenate([key_states, value_states], axis=-1).reshape(row_count, row_width)
    per_dev = row_count // BLOCK_LENGTH
    block_total = kv_size * per_dev
    flattened = chosen.reshape(-1)
    block_ids = jnp.arange(block_total, dtype=jnp.int32)
    present = jnp.any(flattened[:, None] == block_ids[None, :], axis=0).reshape(kv_size, per_dev)
    ranking = jnp.cumsum(present.astype(jnp.int32), axis=1)
    slot_ids = jnp.arange(CAP, dtype=jnp.int32)
    wanted = present[:, :, None] & (ranking[:, :, None] == slot_ids[None, None, :] + 1)
    request = jnp.sum(
        jnp.where(wanted, jnp.arange(per_dev, dtype=jnp.int32)[None, :, None], 0), axis=1
    )
    local_blocks = kv_rows.reshape(per_dev, BLOCK_LENGTH, row_width)
    owners = chosen // per_dev
    within = chosen % per_dev
    slot_of = ranking.reshape(-1)[chosen] - 1
    pool_index = jnp.where(owners == own_index, within, per_dev + owners * CAP + slot_of)
    portion = lax.all_gather(kv_rows, "kv", axis=0, tiled=True)
    owner_count = portion.shape[0] // row_count
    blocks = portion.reshape(owner_count, per_dev, BLOCK_LENGTH, row_width)
    taken = blocks[jnp.arange(owner_count, dtype=jnp.int32)[:, None], request]
    taken = taken.reshape(owner_count * CAP, BLOCK_LENGTH, row_width)
    pool_rows = jnp.concatenate([local_blocks, taken], axis=0)
    selected = pool_rows[pool_index]
    gathered = selected.reshape(per_dev, PICKED_BLOCKS * BLOCK_LENGTH, kv_heads, 2 * HEAD_SIZE)
    sel_keys = gathered[..., :HEAD_SIZE]
    sel_values = gathered[..., HEAD_SIZE:]
    block_queries = query_states.reshape(
        per_dev, BLOCK_LENGTH, kv_heads, group_count_heads, HEAD_SIZE
    )
    sel_scores = (
        jnp.einsum("bqgjd,bkgd->bgjqk", block_queries, sel_keys, preferred_element_type=jnp.float32)
        * score_scale
    )
    key_positions = (
        chosen[:, :, None] * BLOCK_LENGTH + jnp.arange(BLOCK_LENGTH, dtype=jnp.int32)[None, None, :]
    ).reshape(per_dev, PICKED_BLOCKS * BLOCK_LENGTH)
    query_positions = positions.reshape(per_dev, BLOCK_LENGTH)
    allowed = (key_positions[:, None, :] <= query_positions[:, :, None])[:, None, None]
    sel_masked = jnp.where(allowed, sel_scores, NEGATIVE)
    sel_peak = jnp.max(sel_masked, axis=-1, keepdims=True)
    sel_exp = jnp.where(allowed, jnp.exp(sel_masked - sel_peak), 0.0)
    sel_total = jnp.sum(sel_exp, axis=-1, keepdims=True)
    sel_weights = (sel_exp / sel_total).astype(jnp.bfloat16)
    sel_out = jnp.einsum(
        "bgjqk,bkgd->bqgjd", sel_weights, sel_values, preferred_element_type=jnp.float32
    )
    log_sums = jnp.transpose((sel_peak + jnp.log(sel_total))[..., 0], (0, 3, 1, 2)).reshape(
        row_count, head_count
    )
    attended = gate_values[0][:, :, None] * pooled_out.reshape(
        row_count, head_count, HEAD_SIZE
    ) + gate_values[1][:, :, None] * sel_out.reshape(row_count, head_count, HEAD_SIZE)
    attended = attended.astype(jnp.bfloat16).reshape(row_count, head_count * HEAD_SIZE)
    mixed = lax.psum_scatter(
        jnp.dot(attended, out_weight, preferred_element_type=jnp.float32).astype(jnp.bfloat16),
        "tp",
        scatter_dimension=0,
        tiled=True,
    )
    return (mixed, log_sums)


def solution(mesh):
    in_specs = (
        P("kv", None),
        P(None, "tp"),
        P(None, "tp"),
        P(None, "tp"),
        P(),
        P(),
        P(),
        P("tp", None),
        P("kv", None),
    )
    out_specs = (P(("kv", "tp"), None), P("kv", "tp"))
    return jax.shard_map(shards, mesh=mesh, in_specs=in_specs, out_specs=out_specs, check_vma=False)
```

profile of v0, /device:TPU:25, one launch (start us, length us, event | category | flops | bytes accessed | tf_op | source)
XLA Modules:
  0.0 264.0 jit_solution(16780188342533656343)
XLA Ops:
  7.3 0.3 multiply_cosine_fusion
  7.6 0.8 copy.41
  8.3 0.7 copy.42
  9.1 2.6 fusion.70
  11.7 0.8 copy-done.4
  12.5 0.2 reshape.236
  12.7 1.9 fusion.64
  14.7 1.4 subtract_convert_fusion
  16.2 0.6 pad_maximum_fusion.1
  16.8 0.9 copy.68
  17.8 0.1 eq.49
  17.8 0.1 fusion.42
  18.0 0.1 and.22
  18.1 0.1 copy.43
  18.2 0.4 reshape_reshape.11
  18.5 0.2 reduce_window_sum.11
  18.7 0.1 copy.44
  18.8 0.1 reshape.240
  18.9 1.2 reshape_reshape.10
  20.1 4.3 %fusion.71 = f32[256,1024]{0,1:T(8,128)S(1)} fusion(bf16[256,2048]{1,0:T(8,128)(2,1)} %param.9, bf16[2048,1024]{1,0:T(8,128)(2,1)} %param.10), kind=kOutput, calls=%fused_computation.112 | convolution fusion | flops 1073741824 | bytes 6291456 | tf_op jit(solution)/shard_map/reshape | solution.py:50
  24.4 0.1 subtract_convert_fusion.1
  24.5 0.2 concatenate.40
  24.8 1.0 copy.36
  25.8 0.2 concatenate.41
  26.0 1.0 copy.37
  27.0 0.1 select_reduce_fusion
  27.1 0.1 copy.45
  27.2 0.1 reshape.244
  27.3 0.1 reshape.252
  27.4 1.2 gather_fusion.1
  28.8 0.1 reshape.260
  28.8 1.1 copy.48
  30.0 1.1 copy.49
  31.2 0.1 add.182
  31.4 0.2 reshape_reshape.9
  31.6 0.1 multiply_cosine_fusion.1
  31.7 0.4 fusion.27
  32.3 31.3 %all_gather.10 = bf16[256,4,128]{2,0,1:T(8,128)(2,1)S(1)} all-gather(bf16[16,4,128]{2,0,1:T(8,128)(2,1)S(1)} %pad_maximum_fusion.2), channel_id=1, replica_groups=mesh['kv'=16,'tp'=2] {'kv'}, dimensions={0}, use_global_device_ids=true | all-gather | bytes 278528 | tf_op jit(solution)/shard_map/all_gather | solution.py:86
  63.6 0.4 fusion.29
  64.0 34.0 %all_gather.9 = bf16[256,4,128]{2,0,1:T(8,128)(2,1)S(1)} all-gather(bf16[16,4,128]{2,0,1:T(8,128)(2,1)S(1)} %convert_bitcast_fusion), channel_id=1, replica_groups=mesh['kv'=16,'tp'=2] {'kv'}, dimensions={0}, use_global_device_ids=true | all-gather | bytes 278528 | tf_op jit(solution)/shard_map/all_gather | solution.py:87
  98.0 0.1 compare_or_fusion
  98.1 3.7 %fusion.65 = (f32[4,2,256]{2,1,0:T(2,128)S(1)}, f32[4,2,256,256]{2,3,1,0:T(8,128)}) fusion(pred[256,256]{0,1:T(8,128)(4,1)S(1)} %compare_or_fusion, bf16[256,4,2,64]{3,0,2,1:T(8,128)(2,1)} %bitcast.129, bf16[256,4,2,64]{3,0,2,1:T(8,128)(2,1)} %bitcast.128, bf16[256,4,128]{2,0,1:T(8,128)(2,1)S(1)} %all_gather.10), kind=kOutput, calls=%fused_computation.110 | convolution fusion | flops 137888000 | bytes 2957312 | tf_op jit(solution)/shard_map/sub | solution.py:106
  101.8 1.9 fusion.17
  103.7 1.3 copy.39
  105.1 0.4 fusion.11
  105.5 0.1 copy.33
  105.6 0.1 copy.40
  105.8 0.4 broadcast_compare_fusion
  106.2 28.2 %all-gather.2.cloned.1.call-done = bf16[4096,1024]{1,0:T(8,128)(2,1)} async-done(((bf16[256,1024]{1,0:T(8,128)(2,1)}), bf16[4096,1024]{1,0:T(8,128)(2,1)}) %all-gather.2.cloned.1.call-update) | async-done | bytes 8388624 | tf_op jit(solution)/shard_map/all_gather | solution.py:129
  134.3 6.2 %gather_fusion = bf16[32,64,1024]{2,1,0:T(8,128)(2,1)} fusion(bf16[16,4,64,1024]{3,2,1,0:T(8,128)(2,1)} %bitcast.124, s32[32]{0:T(128)S(1)} %reshape.244), kind=kCustom, calls=%fused_computation | custom fusion | bytes 8388864 | tf_op jit(solution)/shard_map/gather | solution.py:132
  140.5 4.7 %pad_maximum_fusion = bf16[36,64,1024]{2,1,0:T(8,128)(2,1)} fusion(bf16[32,64,1024]{2,1,0:T(8,128)(2,1)} %gather_fusion, bf16[4,64,1024]{2,1,0:T(8,128)(2,1)S(1)} %reshape_reshape.11), kind=kLoop, calls=%fused_computation.14 | loop fusion | flops 2359296 | bytes 9437184 | tf_op jit(solution)/shard_map/concatenate | solution.py:134
  145.2 10.8 %gather_fusion.2 = bf16[128,64,1024]{2,1,0:T(8,128)(2,1)} fusion(bf16[36,64,1024]{2,1,0:T(8,128)(2,1)} %pad_maximum_fusion, s32[1024]{0:T(1024)S(1)} %pad_clamp_fusion), kind=kCustom, calls=%fused_computation.2 | custom fusion | bytes 33554944 | tf_op jit(solution)/shard_map/gather | solution.py:135
  156.0 27.9 %reshape.241 = bf16[4,2048,4,256]{3,2,1,0:T(4,128)(2,1)} reshape(bf16[128,64,1024]{2,1,0:T(8,128)(2,1)} %gather_fusion.2) | data formatting | bytes 33554432 | tf_op jit(solution)/shard_map/reshape | solution.py:136
  183.9 15.7 %fusion.63 = (bf16[4,2048,4,128]{3,2,1,0:T(4,128)(2,1)}, bf16[4,2048,4,128]{3,2,1,0:T(4,128)(2,1)}) fusion(bf16[4,2048,4,256]{3,2,1,0:T(4,128)(2,1)} %reshape.241), kind=kLoop, calls=%fused_computation.108 | loop fusion | bytes 33554432 | tf_op jit(solution)/shard_map/slice | solution.py:138
  199.6 16.3 %fusion.1 = (f32[4,4,2,64]{3,2,1,0:T(2,128)S(1)}, f32[4,4,2048,64,2]{2,3,4,1,0:T(8,128)}) fusion(pred[4,64,2048]{2,1,0:T(8,128)(4,1)S(1)} %broadcast_compare_fusion, bf16[4,64,4,2,64]{4,1,3,2,0:T(8,128)(2,1)S(1)} %copy-done.6, bf16[4,64,4,2,64]{4,1,3,2,0:T(8,128)(2,1)S(1)} %copy-done.5, bf16[4,2048,4,128]{3,2,1,0:T(4,128)(2,1)} %get-tuple-element.3), kind=kOutput, calls=%fused_computation.7 | convolution fusion | flops 1087371264 | bytes 26222592 | tf_op jit(solution)/shard_map/bqgjd,bkgd->bgjqk/dot_general | solution.py:143
  216.0 8.8 %fusion.2 = f32[4,4,2,64]{3,2,1,0:T(2,128)S(1)} fusion(f32[4,4,2048,64,2]{2,3,4,1,0:T(8,128)} %get-tuple-element.21, f32[4,4,2,64]{3,2,1,0:T(2,128)S(1)} %get-tuple-element.20, pred[4,64,2048]{2,1,0:T(8,128)(4,1)S(1)} %broadcast_compare_fusion), kind=kLoop, calls=%fused_computation.8 | loop fusion | flops 20969472 | bytes 17317888 | tf_op jit(solution)/shard_map/reduce_sum | solution.py:154
  224.7 10.9 %fusion.7 = f32[4,64,4,2,128]{4,1,3,2,0:T(8,128)} fusion(f32[4,4,2048,64,2]{2,3,4,1,0:T(8,128)} %get-tuple-element.21, f32[4,4,2,64]{3,2,1,0:T(2,128)S(1)} %fusion.2, f32[4,4,2,64]{3,2,1,0:T(2,128)S(1)} %get-tuple-element.20, pred[4,64,2048]{2,1,0:T(8,128)(4,1)S(1)} %broadcast_compare_fusion, bf16[4,2048,4,128]{3,2,1,0:T(4,128)(2,1)S(1)} %copy-done.2), kind=kOutput, calls=%fused_computation.20 | convolution fusion | flops 1098907648 | bytes 26755072 | tf_op jit(solution)/shard_map/bgjqk,bkgd->bqgjd/dot_general | solution.py:156
  235.6 3.1 %copy.50 = f32[4,64,4,2,128]{4,3,2,1,0:T(2,128)} copy(f32[4,64,4,2,128]{4,1,3,2,0:T(8,128)} %fusion.7) | data formatting | bytes 2097152 | tf_op jit(solution)/shard_map/bgjqk,bkgd->bqgjd/transpose | solution.py:156
  238.7 2.1 reshape.242
  240.8 0.3 mul.209
  241.1 0.3 mul.238
  241.5 5.0 %convolution_convert_fusion = bf16[256,2048]{1,0:T(8,128)(2,1)} fusion(bf16[1024,2048]{1,0:T(8,128)(2,1)} %param.16, f32[256,1024]{1,0:T(8,128)S(1)} %reshape.242, f32[32,8,8,128]{3,2,1,0:T(8,128)S(1)} %bitcast.123, f32[256,1024]{1,0:T(8,128)} %copy.39, f32[32,8,8,128]{3,2,1,0:T(8,128)S(1)} %bitcast.122), kind=kOutput, calls=%fused_computation.15 | convolution fusion | flops 1075314688 | bytes 9437184 | tf_op jit(solution)/shard_map/dot_general | solution.py:167
  246.5 0.7 reshape.243
  247.2 10.0 %reduce-scatter.2.cloned.1.call-done = bf16[128,2048]{1,0:T(8,128)(2,1)} async-done(((bf16[256,2048]{1,0:T(8,128)(2,1)}), bf16[128,2048]{1,0:T(8,128)(2,1)}) %reduce-scatter.2.cloned.1.call-update) | async-done | bytes 524304 | tf_op jit(solution)/shard_map/reduce_scatter | solution.py:166
  (52 shorter events, 0.8 us)
Async XLA Ops:
  7.2 5.5 %copy-start = (bf16[2048,512]{1,0:T(8,128)(2,1)S(1)}, bf16[2048,512]{1,0:T(8,128)(2,1)}, u32[]{:S(2)}) copy-start(bf16[2048,512]{1,0:T(8,128)(2,1)} %param.12) | copy-start | bytes 6291460
  7.2 10.6 %copy-start.8 = (s32[4,32]{1,0:T(4,128)S(1)}, s32[4,32]{1,0:T(4,128)}, u32[]{:S(2)}) copy-start(s32[4,32]{1,0:T(4,128)} %param.17) | copy-start | bytes 1540
  7.2 127.1 %all-gather.2.cloned.1.call-start = ((), (), s32[]{:S(2)}) async-start(), calls=%async_computation.1 | async-start | bytes 8912896 | tf_op jit(solution)/shard_map/all_gather | solution.py:129
  11.7 0.8 copy-start.4
  17.7 239.5 %reduce-scatter.2.cloned.1.call-start = ((), (), s32[]{:S(2)}) async-start(), calls=%async_computation.2 | async-start | bytes 1572864 | tf_op jit(solution)/shard_map/reduce_scatter | solution.py:166
  20.1 11.5 %copy-start.9 = (f32[16,8]{0,1:T(8,128)S(1)}, f32[16,8]{0,1:T(8,128)}, u32[]{:S(2)}) copy-start(f32[16,8]{0,1:T(8,128)} %param.14) | copy-start | bytes 1540
  20.1 11.5 %copy-start.10 = (f32[16,8]{0,1:T(8,128)S(1)}, f32[16,8]{0,1:T(8,128)}, u32[]{:S(2)}) copy-start(f32[16,8]{0,1:T(8,128)} %param.15) | copy-start | bytes 1540
  32.1 72.9 %copy-start.3 = (bf16[256,2048]{1,0:T(8,128)(2,1)S(1)}, bf16[256,2048]{1,0:T(8,128)(2,1)}, u32[]{:S(2)}) copy-start(bf16[256,2048]{1,0:T(8,128)(2,1)} %param.9) | copy-start | bytes 3145732
  32.1 72.9 %copy-start.7 = (bf16[2,2048,16]{1,2,0:T(8,128)(2,1)S(1)}, bf16[2,2048,16]{1,2,0:T(8,128)(2,1)}, u32[]{:S(2)}) copy-start(bf16[2,2048,16]{1,2,0:T(8,128)(2,1)} %param.13) | copy-start | bytes 393220
  183.9 15.7 %copy-start.5 = (bf16[4,64,4,2,64]{4,1,3,2,0:T(8,128)(2,1)S(1)}, bf16[4,64,4,2,64]{4,1,3,2,0:T(8,128)(2,1)}, u32[]{:S(2)}) copy-start(bf16[4,64,4,2,64]{4,1,3,2,0:T(8,128)(2,1)} %copy.48) | copy-start | bytes 786436
  183.9 15.7 %copy-start.6 = (bf16[4,64,4,2,64]{4,1,3,2,0:T(8,128)(2,1)S(1)}, bf16[4,64,4,2,64]{4,1,3,2,0:T(8,128)(2,1)}, u32[]{:S(2)}) copy-start(bf16[4,64,4,2,64]{4,1,3,2,0:T(8,128)(2,1)} %copy.49) | copy-start | bytes 786436
  216.0 8.8 %copy-start.2 = (bf16[4,2048,4,128]{3,2,1,0:T(4,128)(2,1)S(1)}, bf16[4,2048,4,128]{3,2,1,0:T(4,128)(2,1)}, u32[]{:S(2)}) copy-start(bf16[4,2048,4,128]{3,2,1,0:T(4,128)(2,1)} %get-tuple-element.2) | copy-start | bytes 25165828
  224.7 32.5 %copy-start.1 = (bf16[2048,512]{1,0:T(8,128)(2,1)S(1)}, bf16[2048,512]{1,0:T(8,128)(2,1)}, u32[]{:S(2)}) copy-start(bf16[2048,512]{1,0:T(8,128)(2,1)} %param.12) | copy-start | bytes 6291460
Sparse Core Ops, SparseCore 0:
  17.8 116.4 all-gather.1
  246.6 10.5 reduce-scatter.1
where the time goes:
time: 266 us; the launch traced here: 264 us
  local copies, waits for them, and re-layouts  81 us (30%)
  blocking collectives  65.3 us (25%)
  matrix products  47.8 us (18%)
  waiting for transfers between devices  38.2 us (14%)
  other arithmetic  17.2 us (6%)
  between operations  14.5 us (5%)
    all_gather x1, blocking collectives, shards(): lax.all_gather(compact_values, 'kv', axis=0, tiled=True)  34 us
    all_gather x1, blocking collectives, shards(): lax.all_gather(compact_keys, 'kv', axis=0, tiled=True)  31.3 us
    all_gather x1, waiting for transfers between devices, shards(): portion = lax.all_gather(kv_rows, 'kv', axis=0, tiled=True)  28.2 us
    reshape x1, local copies, waits for them, and re-layouts, shards(): selected.reshape(per_dev, PICKED_BLOCKS * BLOCK_LENGTH, kv_heads, 2 * HEA...  27.9 us
    dot_general x1, matrix products, shards(): jnp.einsum('bqgjd,bkgd->bgjqk', block_queries, sel_keys, preferred_elemen...  16.3 us
    slice x1, local copies, waits for them, and re-layouts, shards(): sel_values = gathered[..., HEAD_SIZE:]  15.7 us
    dot_general x1, matrix products, shards(): jnp.einsum('bgjqk,bkgd->bqgjd', sel_weights, sel_values, preferred_elemen...  10.9 us
    gather x1, local copies, waits for them, and re-layouts, shards(): selected = pool_rows[pool_index]  10.8 us
  transfers between devices with their start and end apart: 2, of which 2 were waited for; matrix products, arithmetic and copies ran while one was open for 9% of the time, Pallas kernels for 0%

commit v1 on v0

v1 whole, which is shorter than its diff:
```python
import functools
import math

import jax
import jax.numpy as jnp
from jax import lax
from jax.experimental import pallas as pl
from jax.experimental.pallas import tpu as pltpu
from jax.sharding import PartitionSpec as P

HEAD_SIZE = 128
BLOCK_LENGTH = 64
POOL_STRIDE = 16
THETA = 10000.0
NEGATIVE = -1e30
SCALE2 = math.log2(math.e) / math.sqrt(HEAD_SIZE)
LN2 = math.log(2.0)
MESH = pl.DeviceIdType.MESH


def nt(a, b):
    return lax.dot_general(a, b, (((1,), (1,)), ((), ())), preferred_element_type=jnp.float32)


def rotate(x, cosines, sines):
    return x * cosines + pltpu.roll(x, HEAD_SIZE // 2, 1) * sines


def project_kernel(
    r, tokens, wq, wk, wv, gw, cos, sin, cosp, sinp, mixk, mixv, q_out, k_out, v_out, g_out
):
    rows = tokens.shape[0]
    pooled = rows // POOL_STRIDE
    x = tokens[...]
    q = jnp.dot(x, wq[...], preferred_element_type=jnp.float32)
    for j in range(r):
        part = q[:, j * HEAD_SIZE : (j + 1) * HEAD_SIZE]
        q_out[0, :, j * HEAD_SIZE : (j + 1) * HEAD_SIZE] = rotate(part, cos[...], sin[...]).astype(
            jnp.bfloat16
        )
    k = jnp.dot(x, wk[...], preferred_element_type=jnp.float32)
    v = jnp.dot(x, wv[...], preferred_element_type=jnp.float32)
    k_out[0, 0:rows, :] = rotate(k, cos[...], sin[...]).astype(jnp.bfloat16)
    kp = jnp.dot(
        mixk[0], k, preferred_element_type=jnp.float32, precision=lax.Precision.HIGHEST
    )
    vp = jnp.dot(
        mixv[0], v, preferred_element_type=jnp.float32, precision=lax.Precision.HIGHEST
    )
    k_out[0, rows : rows + pooled, :] = rotate(kp, cosp[...], sinp[...]).astype(jnp.bfloat16)
    k_out[0, rows + pooled : rows + 2 * pooled, :] = vp.astype(jnp.bfloat16)
    v_out[0] = v.T.astype(jnp.bfloat16)

    @pl.when(pl.program_id(0) == 0)
    def _():
        heads = gw.shape[2]
        for b in range(2):
            logits = lax.dot_general(
                gw[b], x, (((0,), (1,)), ((), ())), preferred_element_type=jnp.float32
            )
            g_out[b * heads : (b + 1) * heads, :] = jax.nn.sigmoid(logits)


def attend_kernel(
    dims,
    q_in,
    k_in,
    v_in,
    cnt_in,
    g_in,
    wo_in,
    mixed,
    lse_out,
    qbuf,
    kbuf,
    vbuf,
    cbuf,
    gbuf,
    wo,
    bias_ref,
    acc,
    mref,
    lref,
    pacc,
    pmref,
    plref,
    obox,
    lbox,
    abuf,
    lbuf,
    sbox,
    rbox,
    local_sem,
    send_sem,
    recv_sem,
    chain_send,
    chain_recv,
    back_send,
    back_recv,
    tp_send,
    tp_recv,
):
    G, Z, T, R, r, H = dims
    nb = G * (R // BLOCK_LENGTH)
    pooled = R // POOL_STRIDE
    kv = lax.axis_index("kv")
    t = lax.axis_index("tp")
    c = lax.rem(kv, G)
    z = kv // G

    def member(g):
        return lax.rem(c + g, G)

    def at(group, who):
        return {"kv": group * G + who}

    barrier = pltpu.get_barrier_semaphore()
    for g in range(1, G):
        pl.semaphore_signal(barrier, inc=1, device_id=at(z, member(g)), device_id_type=MESH)
    for d in (1, Z - 1):
        pl.semaphore_signal(
            barrier, inc=1, device_id=at(lax.rem(z + d, Z), c), device_id_type=MESH
        )
    for o in range(1, T):
        pl.semaphore_signal(
            barrier, inc=1, device_id={"tp": lax.rem(t + o, T)}, device_id_type=MESH
        )
    wo_copy = pltpu.make_async_copy(wo_in, wo, local_sem.at[5])
    wo_copy.start()
    locals_ = [
        pltpu.make_async_copy(k_in.at[c], kbuf.at[0, c], local_sem.at[0]),
        pltpu.make_async_copy(v_in.at[c], vbuf.at[0, c], local_sem.at[1]),
        pltpu.make_async_copy(q_in.at[c], qbuf.at[c], local_sem.at[2]),
        pltpu.make_async_copy(cnt_in, cbuf.at[c], local_sem.at[3]),
        pltpu.make_async_copy(g_in, gbuf.at[c], local_sem.at[4]),
    ]
    for copy in locals_:
        copy.start()
    pl.semaphore_wait(barrier, G - 1 + 2 + T - 1)

    swaps = []
    for i in range(5):
        for g in range(1, G):
            who = member(g)
            src, dst = [
                (k_in.at[who], kbuf.at[0, c]),
                (v_in.at[who], vbuf.at[0, c]),
                (q_in.at[who], qbuf.at[c]),
                (cnt_in, cbuf.at[c]),
                (g_in, gbuf.at[c]),
            ][i]
            copy = pltpu.make_async_remote_copy(
                src_ref=src,
                dst_ref=dst,
                send_sem=send_sem.at[i, g],
                recv_sem=recv_sem.at[i, g],
                device_id=at(z, who),
                device_id_type=MESH,
            )
            copy.start()
            swaps.append(copy)

    def chain(s):
        up = at(lax.rem(z + 1, Z), c)
        return [
            pltpu.make_async_remote_copy(
                src_ref=buf.at[s],
                dst_ref=buf.at[s + 1],
                send_sem=chain_send.at[i, s],
                recv_sem=chain_recv.at[i, s],
                device_id=up,
                device_id_type=MESH,
            )
            for i, buf in ((0, kbuf), (1, vbuf))
        ]

    for copy in locals_[:2]:
        copy.wait()
    for copy in swaps[: 2 * (G - 1)]:
        copy.wait_recv()

    @pl.when(z + 1 < Z)
    def _():
        for copy in chain(0):
            copy.start()

    for copy in locals_[2:]:
        copy.wait()
    for copy in swaps[2 * (G - 1) :]:
        copy.wait_recv()

    lanes_q = lax.broadcasted_iota(jnp.int32, (128, R), 1) // BLOCK_LENGTH
    spread = (lanes_q == lax.broadcasted_iota(jnp.int32, (128, R), 0)).astype(jnp.bfloat16)

    def make_bias(n, carry):
        who, plane = n // Z, lax.rem(n, Z)
        counts = jnp.dot(
            cbuf[who, plane].astype(jnp.bfloat16), spread, preferred_element_type=jnp.float32
        )
        bias_ref[who, plane] = jnp.where(
            counts > 0.5, jnp.log2(jnp.maximum(counts, 1.0)), NEGATIVE
        )
        return carry

    lax.fori_loop(0, G * Z, make_bias, 0)

    def attend(s, first):
        plane = z - s

        def chunk(n, carry):
            cq, j = n // r, lax.rem(n, r)
            q = qbuf[cq, :, pl.ds(pl.multiple_of(j * HEAD_SIZE, HEAD_SIZE), HEAD_SIZE)]
            bias = bias_ref[cq, plane]
            st = jnp.concatenate([nt(kbuf[s, a, 0:R, :], q) for a in range(G)], axis=0) * SCALE2
            st = st.reshape(nb, BLOCK_LENGTH, R) + bias[:nb].reshape(nb, 1, R)
            st = st.reshape(G * R, R)
            if first:
                keys = lax.broadcasted_iota(jnp.int32, (G * R, R), 0)
                queries = lax.broadcasted_iota(jnp.int32, (G * R, R), 1) + cq * R
                st = jnp.where(keys <= queries, st, NEGATIVE)
            kp = kbuf[s, :, R : R + pooled, :].reshape(G * pooled, HEAD_SIZE)
            vp = kbuf[s, :, R + pooled : R + 2 * pooled, :].reshape(G * pooled, HEAD_SIZE)
            index = plane * (G * pooled) + lax.broadcasted_iota(jnp.int32, (G * pooled, R), 0)
            where_q = (z * G + cq) * R + lax.broadcasted_iota(jnp.int32, (G * pooled, R), 1)
            seen = (POOL_STRIDE * index + POOL_STRIDE - 1 <= where_q) | (index == 0)
            sp = jnp.where(seen, nt(kp, q) * SCALE2, NEGATIVE)
            peak = jnp.max(st, axis=0, keepdims=True)
            ppeak = jnp.max(sp, axis=0, keepdims=True)
            if not first:
                peak = jnp.maximum(peak, mref[cq, j])
                ppeak = jnp.maximum(ppeak, pmref[cq, j])
            e = jnp.exp2(st - peak)
            pe = jnp.exp2(sp - ppeak)
            total = jnp.sum(e, axis=0, keepdims=True)
            ptotal = jnp.sum(pe, axis=0, keepdims=True)
            eb = e.astype(jnp.bfloat16)
            out = jnp.dot(vbuf[s, 0], eb[0:R], preferred_element_type=jnp.float32)
            for a in range(1, G):
                out += jnp.dot(
                    vbuf[s, a], eb[a * R : (a + 1) * R], preferred_element_type=jnp.float32
                )
            pout = lax.dot_general(
                vp,
                pe.astype(jnp.bfloat16),
                (((0,), (0,)), ((), ())),
                preferred_element_type=jnp.float32,
            )
            if not first:
                shrink = jnp.exp2(mref[cq, j] - peak)
                pshrink = jnp.exp2(pmref[cq, j] - ppeak)
                total += lref[cq, j] * shrink
                ptotal += plref[cq, j] * pshrink
                out += acc[cq, j] * shrink
                pout += pacc[cq, j] * pshrink
            mref[cq, j] = peak
            lref[cq, j] = total
            acc[cq, j] = out
            pmref[cq, j] = ppeak
            plref[cq, j] = ptotal
            pacc[cq, j] = pout
            return carry

        lax.fori_loop(0, G * r, chunk, 0)

    attend(0, True)

    def step(s, carry):
        for copy in chain(s - 1):
            copy.wait_recv()

        @pl.when(z + 1 < Z)
        def _():
            for copy in chain(s):
                copy.start()

        attend(s, False)
        return carry

    lax.fori_loop(1, z + 1, step, 0)

    backs = []
    for g in list(range(1, G)) + [0]:
        who = member(g)
        for j in range(r):
            head = t * (G * r) + c * r + j
            gate_p = gbuf[who, pl.ds(head, 1), :]
            gate_s = gbuf[who, pl.ds(H + head, 1), :]
            total = lref[who, j]
            mixed_t = pacc[who, j] * (gate_p / plref[who, j]) + acc[who, j] * (gate_s / total)
            obox[g, :, j * HEAD_SIZE : (j + 1) * HEAD_SIZE] = mixed_t.T.astype(jnp.bfloat16)
            lbox[g, j : j + 1, :] = (mref[who, j] + jnp.log2(total)) * LN2
        if g:
            for i, (src, dst) in enumerate(((obox.at[g], abuf.at[c]), (lbox.at[g], lbuf.at[c]))):
                copy = pltpu.make_async_remote_copy(
                    src_ref=src,
                    dst_ref=dst,
                    send_sem=back_send.at[i, g],
                    recv_sem=back_recv.at[i, g],
                    device_id=at(z, who),
                    device_id_type=MESH,
                )
                copy.start()
                backs.append(copy)
    abuf[c] = obox[0]
    lbuf[c] = lbox[0]
    wo_copy.wait()
    for copy in backs:
        copy.wait_recv()
    lse_out[...] = lbuf[...]

    width = wo.shape[1]
    piece = R // T
    span = r * HEAD_SIZE

    def share(dest):
        rows = pl.ds(pl.multiple_of(dest * piece, piece), piece)
        total = None
        for a in range(G):
            term = jnp.dot(
                abuf[a, rows, :],
                wo[a * span : (a + 1) * span, :],
                preferred_element_type=jnp.float32,
            )
            total = term if total is None else total + term
        return total.astype(jnp.bfloat16)

    hops = []
    for o in range(1, T):
        dest = lax.rem(t + o, T)
        sbox[o] = share(dest)
        copy = pltpu.make_async_remote_copy(
            src_ref=sbox.at[o],
            dst_ref=rbox.at[o],
            send_sem=tp_send.at[o],
            recv_sem=tp_recv.at[o],
            device_id={"tp": dest},
            device_id_type=MESH,
        )
        copy.start()
        hops.append(copy)
    final = share(t).astype(jnp.float32)
    for o in range(1, T):
        hops[o - 1].wait_recv()
        final = final + rbox[o].astype(jnp.float32)
    mixed[...] = final.astype(jnp.bfloat16)

    for copy in swaps + backs + hops:
        copy.wait_send()

    @pl.when(z + 1 < Z)
    def _():
        def drain(s, carry):
            for copy in chain(s):
                copy.wait_send()
            return carry

        lax.fori_loop(0, z + 1, drain, 0)


def shards(
    tokens,
    query_weight,
    key_matrix,
    value_matrix,
    gate_weight,
    key_pool_weight,
    value_pool_weight,
    out_weight,
    chosen,
):
    R, width = tokens.shape
    kv_size = lax.axis_size("kv")
    T = lax.axis_size("tp")
    kv = lax.axis_index("kv")
    t = lax.axis_index("tp")
    G = key_matrix.shape[1] // HEAD_SIZE
    r = query_weight.shape[1] // key_matrix.shape[1]
    Z = kv_size // G
    H = gate_weight.shape[2]
    per_dev = chosen.shape[0]
    pooled = R // POOL_STRIDE
    nb = G * per_dev
    nbp = max(8, nb)
    span = r * HEAD_SIZE
    f32, bf16 = jnp.float32, jnp.bfloat16

    half = HEAD_SIZE // 2
    lane = jnp.arange(HEAD_SIZE, dtype=jnp.int32)
    inverse = THETA ** (-(lane % half).astype(f32) / half)
    positions = kv * R + jnp.arange(R, dtype=jnp.int32)
    angles = positions.astype(f32)[:, None] * inverse[None, :]
    cos = jnp.cos(angles)
    sin = jnp.sin(angles) * jnp.where(lane < half, -1.0, 1.0)[None, :]
    cosp = cos[POOL_STRIDE - 1 :: POOL_STRIDE]
    sinp = sin[POOL_STRIDE - 1 :: POOL_STRIDE]

    own = jnp.arange(R)[None, :] // POOL_STRIDE == jnp.arange(pooled)[:, None]

    def mixer(weights):
        mine = lax.dynamic_slice_in_dim(weights, t * G, G, 1).T
        return jnp.where(own[None], jnp.tile(mine, (1, pooled))[:, None, :], 0.0)

    once = lambda *shape: pl.BlockSpec(shape, lambda g: (0,) * len(shape))
    q_all, k_all, v_all, gates = pl.pallas_call(
        functools.partial(project_kernel, r),
        grid=(G,),
        in_specs=[
            once(R, width),
            pl.BlockSpec((width, span), lambda g: (0, g)),
            pl.BlockSpec((width, HEAD_SIZE), lambda g: (0, g)),
            pl.BlockSpec((width, HEAD_SIZE), lambda g: (0, g)),
            once(2, width, H),
            once(R, HEAD_SIZE),
            once(R, HEAD_SIZE),
            once(pooled, HEAD_SIZE),
            once(pooled, HEAD_SIZE),
            pl.BlockSpec((1, pooled, R), lambda g: (g, 0, 0)),
            pl.BlockSpec((1, pooled, R), lambda g: (g, 0, 0)),
        ],
        out_specs=[
            pl.BlockSpec((1, R, span), lambda g: (g, 0, 0)),
            pl.BlockSpec((1, R + 2 * pooled, HEAD_SIZE), lambda g: (g, 0, 0)),
            pl.BlockSpec((1, HEAD_SIZE, R), lambda g: (g, 0, 0)),
            once(2 * H, R),
        ],
        out_shape=[
            jax.ShapeDtypeStruct((G, R, span), bf16),
            jax.ShapeDtypeStruct((G, R + 2 * pooled, HEAD_SIZE), bf16),
            jax.ShapeDtypeStruct((G, HEAD_SIZE, R), bf16),
            jax.ShapeDtypeStruct((2 * H, R), f32),
        ],
        name="project",
    )(
        tokens,
        query_weight,
        key_matrix,
        value_matrix,
        gate_weight,
        cos,
        sin,
        cosp,
        sinp,
        mixer(key_pool_weight),
        mixer(value_pool_weight),
    )

    blocks = jnp.arange(kv_size * per_dev, dtype=jnp.int32)
    counts = jnp.sum((chosen[None] == blocks[:, None, None]).astype(f32), axis=2)
    counts = jnp.pad(counts.reshape(Z, nb, per_dev), ((0, 0), (0, nbp - nb), (0, 128 - per_dev)))

    vmem = pl.BlockSpec(memory_space=pltpu.VMEM)
    anywhere = pl.BlockSpec(memory_space=pl.ANY)
    sem = pltpu.SemaphoreType.DMA
    mixed, lse = pl.pallas_call(
        functools.partial(attend_kernel, (G, Z, T, R, r, H)),
        in_specs=[anywhere] * 6,
        out_specs=[vmem, vmem],
        out_shape=[
            jax.ShapeDtypeStruct((R // T, out_weight.shape[1]), bf16),
            jax.ShapeDtypeStruct((G, 8, R), f32),
        ],
        scratch_shapes=[
            pltpu.VMEM((G, R, span), bf16),
            pltpu.VMEM((Z, G, R + 2 * pooled, HEAD_SIZE), bf16),
            pltpu.VMEM((Z, G, HEAD_SIZE, R), bf16),
            pltpu.VMEM((G, Z, nbp, 128), f32),
            pltpu.VMEM((G, 2 * H, R), f32),
            pltpu.VMEM(out_weight.shape, bf16),
            pltpu.VMEM((G, Z, nbp, R), f32),
            pltpu.VMEM((G, r, HEAD_SIZE, R), f32),
            pltpu.VMEM((G, r, 1, R), f32),
            pltpu.VMEM((G, r, 1, R), f32),
            pltpu.VMEM((G, r, HEAD_SIZE, R), f32),
            pltpu.VMEM((G, r, 1, R), f32),
            pltpu.VMEM((G, r, 1, R), f32),
            pltpu.VMEM((G, R, span), bf16),
            pltpu.VMEM((G, 8, R), f32),
            pltpu.VMEM((G, R, span), bf16),
            pltpu.VMEM((G, 8, R), f32),
            pltpu.VMEM((T, R // T, out_weight.shape[1]), bf16),
            pltpu.VMEM((T, R // T, out_weight.shape[1]), bf16),
            sem((6,)),
            sem((5, G)),
            sem((5, G)),
            sem((2, Z)),
            sem((2, Z)),
            sem((2, G)),
            sem((2, G)),
            sem((T,)),
            sem((T,)),
        ],
        compiler_params=pltpu.CompilerParams(collective_id=0, has_side_effects=True),
        name="attend",
    )(q_all, k_all, v_all, counts, gates, out_weight)
    log_sums = lse[:, :r, :].reshape(G * r, R).T
    return mixed, log_sums


def solution(mesh):
    in_specs = (
        P("kv", None),
        P(None, "tp"),
        P(None, "tp"),
        P(None, "tp"),
        P(),
        P(),
        P(),
        P("tp", None),
        P("kv", None),
    )
    out_specs = (P(("kv", "tp"), None), P("kv", "tp"))
    return jax.shard_map(shards, mesh=mesh, in_specs=in_specs, out_specs=out_specs, check_vma=False)
```

time: 266 us -> 88.1 us (0.33)
  Pallas kernels: 0 us -> 77.4 us
  local copies, waits for them, and re-layouts: 81 us -> 8.36 us
  blocking collectives: 65.3 us -> 0 us
  matrix products: 47.8 us -> 0 us
  waiting for transfers between devices: 38.2 us -> 0 us
  other arithmetic: 17.2 us -> 1.33 us
  between operations: 14.5 us -> 0.69 us
    pallas_call x0 -> x2, Pallas kernels: none -> 77.4 us  [the longest x1 68.1 us: shards(): pl.pallas_call(functools.partial(attend_kernel, (G, Z, T, R, r, H)), in_s...]
    all_gather x2 -> x0, blocking collectives: 65.3 us -> none  [the longest x1 34 us: shards(): lax.all_gather(compact_values, 'kv', axis=0, tiled=True)]
    dot_general x9 -> x0, matrix products: 39.9 us -> none  [the longest x1 16.3 us: shards(): jnp.einsum('bqgjd,bkgd->bgjqk', block_queries, sel_keys, preferred_elemen...]
    reshape x6 -> x1, local copies, waits for them, and re-layouts: 32.2 us -> 0.61 us  [shards(): log_sums = lse[:, :r, :].reshape(G * r, R).T]
    all_gather x1 -> x0, waiting for transfers between devices: 28.2 us -> none  [shards(): portion = lax.all_gather(kv_rows, 'kv', axis=0, tiled=True)]
    gather x3 -> x0, local copies, waits for them, and re-layouts: 18.2 us -> none  [the longest x1 10.8 us: shards(): selected = pool_rows[pool_index]]
    slice x1 -> x3, local copies, waits for them, and re-layouts: 15.7 us -> 2.02 us  [the longest x1 0.76 us: shards(): log_sums = lse[:, :r, :].reshape(G * r, R).T]
    reduce_scatter x1 -> x0, waiting for transfers between devices: 9.99 us -> none  [shards(): lax.psum_scatter(jnp.dot(attended, out_weight, preferred_element_type=jnp...]
  transfers between devices with their start and end apart: 2 -> 0, of which waited for: 2 -> 0; matrix products, arithmetic and copies ran while one was open for 9% -> 0% of each run, Pallas kernels for 0% -> 0%
where the time goes in v1:
time: 88.1 us; the launch traced here: 87.8 us
  Pallas kernels  77.4 us (88%)
  local copies, waits for them, and re-layouts  8.36 us (9%)
  other arithmetic  1.33 us (2%)
    pallas_call x1, Pallas kernels, shards(): pl.pallas_call(functools.partial(attend_kernel, (G, Z, T, R, r, H)), in_s...  68.1 us
    pallas_call x1, Pallas kernels, shards(): pl.pallas_call(functools.partial(project_kernel, r), grid=(G,), in_specs=...  9.29 us
    unnamed x8, local copies, waits for them, and re-layouts  4.11 us

profile of v1, /device:TPU:25, one launch (start us, length us, event | category | flops | bytes accessed | tf_op | source)
XLA Modules:
  0.0 87.8 jit_solution(1096346327799372809)
XLA Ops:
  0.6 0.7 dynamic-slice_bitcast_fusion
  1.4 0.1 tile.17
  1.4 0.1 tile.19
  1.5 0.7 broadcast_select_fusion
  2.2 0.5 fusion
  2.8 0.0 copy-start
  2.8 0.0 copy-start.1
  2.8 0.7 slice.10.sinp
  3.4 0.6 slice.9.cosp
  4.1 2.2 %copy.12.gw = bf16[2,2048,16]{2,1,0:T(8,128)(2,1)} copy(bf16[2,2048,16]{1,2,0:T(8,128)(2,1)} %param.13) | data formatting | bytes 262144 | tf_op args[4]
  6.3 0.0 copy-done
  6.3 0.0 copy-done.1
  6.3 0.0 copy-start.2
  6.3 9.3 %project.1 = (bf16[4,256,256]{2,1,0:T(8,128)(2,1)}, bf16[4,288,128]{2,1,0:T(8,128)(2,1)}, bf16[4,128,256]{2,1,0:T(8,128)(2,1)}, f32[32,256]{1,0:T(8,128)}) custom-call(bf16[256,2048]{1,0:T(8,128)(2,1)} %tokens.1, bf16[2048,1024]{1,0:T(8,128)(2,1)} %wq.1, bf16[2048,512]{1,0:T(8,128)(2,1)} %wk.1, bf16[2048,512]{1,0:T(8,128)(2,1)} %wv.1, ...), custom_call_target="tpu_custom_call" | custom-call | tf_op jit(solution)/shard_map/project/pallas_call | solution.py:404
  15.6 0.0 copy-done.2
  15.6 0.1 convert_reduce_fusion
  15.7 0.1 copy.13
  15.8 0.6 pad.4.cnt_in
  16.4 68.1 %attend.1 = (bf16[128,2048]{1,0:T(8,128)(2,1)}, f32[4,8,256]{2,1,0:T(8,128)}) custom-call(bf16[4,256,256]{2,1,0:T(8,128)(2,1)} %get-tuple-element.8.q_in, bf16[4,288,128]{2,1,0:T(8,128)(2,1)} %get-tuple-element.9.k_in, bf16[4,128,256]{2,1,0:T(8,128)(2,1)} %get-tuple-element.10.v_in, f32[4,16,128]{2,1,0:T(8,128)} %pad.4.cnt_in, ...), custom_call_target="tpu_custom_call" | custom-call | tf_op jit(solution)/shard_map/attend/pallas_call | solution.py:454
  84.5 0.8 slice.11
  85.3 0.6 reshape.104
  85.9 1.9 %copy.15 = bf16[128,2048]{1,0:T(8,128)(2,1)} copy(bf16[128,2048]{1,0:T(8,128)(2,1)} %get-tuple-element.24) | data formatting | bytes 1048576
  (6 shorter events, 0.0 us)
Async XLA Ops:
  2.8 3.5 %copy-start = (f32[256,128]{1,0:T(8,128)}, f32[256,128]{1,0:T(8,128)S(1)}, u32[]{:S(2)}) copy-start(f32[256,128]{1,0:T(8,128)S(1)} %get-tuple-element.16.sin) | copy-start | bytes 393220
  2.8 3.5 %copy-start.1 = (f32[256,128]{1,0:T(8,128)}, f32[256,128]{1,0:T(8,128)S(1)}, u32[]{:S(2)}) copy-start(f32[256,128]{1,0:T(8,128)S(1)} %get-tuple-element.17.cos) | copy-start | bytes 393220
  6.3 9.3 %copy-start.2 = (s32[4,32]{1,0:T(4,128)S(1)}, s32[4,32]{1,0:T(4,128)}, u32[]{:S(2)}) copy-start(s32[4,32]{1,0:T(4,128)} %param.17) | copy-start | bytes 1540

commit v2 on v1

v2 whole, which is shorter than its diff:
```python
import functools
import math

import jax
import jax.numpy as jnp
from jax import lax
from jax.experimental import pallas as pl
from jax.experimental.pallas import tpu as pltpu
from jax.sharding import PartitionSpec as P

HEAD_SIZE = 128
BLOCK_LENGTH = 64
POOL_STRIDE = 16
THETA = 10000.0
NEGATIVE = -1e30
SCALE2 = math.log2(math.e) / math.sqrt(HEAD_SIZE)
LN2 = math.log(2.0)
MESH = pl.DeviceIdType.MESH


def nt(a, b):
    return lax.dot_general(a, b, (((1,), (1,)), ((), ())), preferred_element_type=jnp.float32)


def rotate(x, cosines, sines):
    return x * cosines + pltpu.roll(x, HEAD_SIZE // 2, 1) * sines


def pool_matrix(weights, head, rows):
    pooled = rows // POOL_STRIDE
    row = weights[pl.ds(head, 1), :]
    shape = (POOL_STRIDE, POOL_STRIDE)
    eye = lax.broadcasted_iota(jnp.int32, shape, 0) == lax.broadcasted_iota(jnp.int32, shape, 1)
    column = jnp.sum(jnp.where(eye, row, 0.0), axis=1, keepdims=True)
    wide = (POOL_STRIDE, rows)
    match = lax.broadcasted_iota(jnp.int32, wide, 0) == lax.rem(
        lax.broadcasted_iota(jnp.int32, wide, 1), POOL_STRIDE
    )
    tiled = jnp.sum(jnp.where(match, column, 0.0), axis=0, keepdims=True)
    tall = (pooled, rows)
    own = lax.broadcasted_iota(jnp.int32, tall, 0) == (
        lax.broadcasted_iota(jnp.int32, tall, 1) // POOL_STRIDE
    )
    return jnp.where(own, tiled, 0.0)


def attend_kernel(
    dims,
    x_in,
    wq_in,
    wk_in,
    wv_in,
    wo_in,
    cnt_in,
    gw,
    kpool,
    vpool,
    cos,
    sin,
    mixed,
    lse_out,
    x,
    wq,
    wkv,
    wo,
    qst,
    kst,
    vst,
    gst,
    qbuf,
    kbuf,
    vbuf,
    cbuf,
    gbuf,
    bias_ref,
    acc,
    mref,
    lref,
    pacc,
    pmref,
    plref,
    obox,
    lbox,
    abuf,
    lbuf,
    sbox,
    rbox,
    local_sem,
    weight_sem,
    send_sem,
    recv_sem,
    chain_send,
    chain_recv,
    back_send,
    back_recv,
    tp_send,
    tp_recv,
):
    G, Z, T, R, r, H = dims
    nb = G * (R // BLOCK_LENGTH)
    pooled = R // POOL_STRIDE
    span = r * HEAD_SIZE
    kv = lax.axis_index("kv")
    t = lax.axis_index("tp")
    c = lax.rem(kv, G)
    z = kv // G

    def member(g):
        return lax.rem(c + g, G)

    def at(group, who):
        return {"kv": group * G + who}

    barrier = pltpu.get_barrier_semaphore()
    for g in range(1, G):
        pl.semaphore_signal(barrier, inc=1, device_id=at(z, member(g)), device_id_type=MESH)
    for d in (1, Z - 1):
        pl.semaphore_signal(
            barrier, inc=1, device_id=at(lax.rem(z + d, Z), c), device_id_type=MESH
        )
    for o in range(1, T):
        pl.semaphore_signal(
            barrier, inc=1, device_id={"tp": lax.rem(t + o, T)}, device_id_type=MESH
        )

    x_copy = pltpu.make_async_copy(x_in, x, local_sem.at[0])
    x_copy.start()
    key_copies, query_copies = [], []
    for g in range(G):
        cols = pl.ds(pl.multiple_of(member(g) * HEAD_SIZE, HEAD_SIZE), HEAD_SIZE)
        pair = (
            pltpu.make_async_copy(
                wk_in.at[:, cols], wkv.at[g, :, pl.ds(0, HEAD_SIZE)], weight_sem.at[0, g]
            ),
            pltpu.make_async_copy(
                wv_in.at[:, cols], wkv.at[g, :, pl.ds(HEAD_SIZE, HEAD_SIZE)], weight_sem.at[1, g]
            ),
        )
        for copy in pair:
            copy.start()
        key_copies.append(pair)
    for g in list(range(1, G)) + [0]:
        cols = pl.ds(pl.multiple_of(member(g) * span, span), span)
        copy = pltpu.make_async_copy(wq_in.at[:, cols], wq.at[g], weight_sem.at[2, g])
        copy.start()
        query_copies.append(copy)
    cnt_copy = pltpu.make_async_copy(cnt_in, cbuf.at[c], local_sem.at[1])
    cnt_copy.start()
    wo_copy = pltpu.make_async_copy(wo_in, wo, local_sem.at[2])
    wo_copy.start()

    def swap(i, g):
        src, dst = [
            (kst.at[g], kbuf.at[0, c]),
            (vst.at[g], vbuf.at[0, c]),
            (qst.at[g], qbuf.at[c]),
            (cnt_in, cbuf.at[c]),
            (gst, gbuf.at[c]),
        ][i]
        return pltpu.make_async_remote_copy(
            src_ref=src,
            dst_ref=dst,
            send_sem=send_sem.at[i, g],
            recv_sem=recv_sem.at[i, g],
            device_id=at(z, member(g)),
            device_id_type=MESH,
        )

    def chain(s, g):
        up = at(lax.rem(z + 1, Z), c)
        source = lax.rem(c + G - g, G)
        return [
            pltpu.make_async_remote_copy(
                src_ref=buf.at[s, source],
                dst_ref=buf.at[s + 1, source],
                send_sem=chain_send.at[i, s, g],
                recv_sem=chain_recv.at[i, s, g],
                device_id=up,
                device_id_type=MESH,
            )
            for i, buf in ((0, kbuf), (1, vbuf))
        ]

    def forward(s, g):
        @pl.when(z + 1 < Z)
        def _():
            for copy in chain(s, g):
                copy.start()

    def pass_on(s, g):
        @pl.when(s <= z)
        def _():
            for copy in chain(s - 1, g):
                copy.wait_recv()
            forward(s, g)

    pl.semaphore_wait(barrier, G - 1 + 2 + T - 1)
    x_copy.wait()
    for g in range(G):
        for copy in key_copies[g]:
            copy.wait()
        head = t * G + member(g)
        both = jnp.dot(x[...], wkv[g], preferred_element_type=jnp.float32)
        k, v = both[:, :HEAD_SIZE], both[:, HEAD_SIZE:]
        kp = jnp.dot(
            pool_matrix(kpool, head, R),
            k,
            preferred_element_type=jnp.float32,
            precision=lax.Precision.HIGHEST,
        )
        vp = jnp.dot(
            pool_matrix(vpool, head, R),
            v,
            preferred_element_type=jnp.float32,
            precision=lax.Precision.HIGHEST,
        )
        ends = pl.ds(POOL_STRIDE - 1, pooled, stride=POOL_STRIDE)
        rows_k = rotate(k, cos[...], sin[...]).astype(jnp.bfloat16)
        rows_p = rotate(kp, cos[ends, :], sin[ends, :]).astype(jnp.bfloat16)
        k_to, v_to = (kbuf.at[0, c], vbuf.at[0, c]) if g == 0 else (kst.at[g], vst.at[g])
        k_to[0:R, :] = rows_k
        k_to[R : R + pooled, :] = rows_p
        k_to[R + pooled : R + 2 * pooled, :] = vp.astype(jnp.bfloat16)
        v_to[...] = v.T.astype(jnp.bfloat16)
        if g == 0:
            forward(0, 0)
        else:
            swap(0, g).start()
            swap(1, g).start()
    for n, g in enumerate(list(range(1, G)) + [0]):
        query_copies[n].wait()
        q = jnp.dot(x[...], wq[g], preferred_element_type=jnp.float32)
        q_to = qst.at[g] if g else qbuf.at[c]
        for j in range(r):
            cols = slice(j * HEAD_SIZE, (j + 1) * HEAD_SIZE)
            q_to[:, cols] = rotate(q[:, cols], cos[...], sin[...]).astype(jnp.bfloat16)
        if g:
            swap(2, g).start()
            swap(0, g).wait_recv()
            swap(1, g).wait_recv()
            forward(0, g)
    for b in range(2):
        gst[b * H : (b + 1) * H, :] = jax.nn.sigmoid(nt(gw[b], x[...]))
    gbuf[c] = gst[...]
    for i in (3, 4):
        for g in range(1, G):
            swap(i, g).start()
    cnt_copy.wait()
    early = G // 2
    for g in range(early):
        pass_on(1, g)
    for i in (2, 3, 4):
        for g in range(1, G):
            swap(i, g).wait_recv()

    lanes_q = lax.broadcasted_iota(jnp.int32, (128, R), 1) // BLOCK_LENGTH
    spread = (lanes_q == lax.broadcasted_iota(jnp.int32, (128, R), 0)).astype(jnp.bfloat16)

    def make_bias(n, carry):
        who, plane = n // Z, lax.rem(n, Z)
        counts = jnp.dot(
            cbuf[who, plane].astype(jnp.bfloat16), spread, preferred_element_type=jnp.float32
        )
        bias_ref[who, plane] = jnp.where(
            counts > 0.5, jnp.log2(jnp.maximum(counts, 1.0)), NEGATIVE
        )
        return carry

    lax.fori_loop(0, G * Z, make_bias, 0)

    def chunk(s, first, cq, j):
        plane = z - s
        q = qbuf[cq, :, j * HEAD_SIZE : (j + 1) * HEAD_SIZE]
        bias = bias_ref[cq, plane]
        st = jnp.concatenate([nt(kbuf[s, a, 0:R, :], q) for a in range(G)], axis=0) * SCALE2
        st = st.reshape(nb, BLOCK_LENGTH, R) + bias[:nb].reshape(nb, 1, R)
        st = st.reshape(G * R, R)
        if first:
            keys = lax.broadcasted_iota(jnp.int32, (G * R, R), 0)
            queries = lax.broadcasted_iota(jnp.int32, (G * R, R), 1) + cq * R
            st = jnp.where(keys <= queries, st, NEGATIVE)
        kp = kbuf[s, :, R : R + pooled, :].reshape(G * pooled, HEAD_SIZE)
        vp = kbuf[s, :, R + pooled : R + 2 * pooled, :].reshape(G * pooled, HEAD_SIZE)
        index = plane * (G * pooled) + lax.broadcasted_iota(jnp.int32, (G * pooled, R), 0)
        where_q = (z * G + cq) * R + lax.broadcasted_iota(jnp.int32, (G * pooled, R), 1)
        seen = (POOL_STRIDE * index + POOL_STRIDE - 1 <= where_q) | (index == 0)
        sp = jnp.where(seen, nt(kp, q) * SCALE2, NEGATIVE)
        peak = jnp.max(st, axis=0, keepdims=True)
        ppeak = jnp.max(sp, axis=0, keepdims=True)
        if not first:
            peak = jnp.maximum(peak, mref[cq, j])
            ppeak = jnp.maximum(ppeak, pmref[cq, j])
        e = jnp.exp2(st - peak)
        pe = jnp.exp2(sp - ppeak)
        total = jnp.sum(e, axis=0, keepdims=True)
        ptotal = jnp.sum(pe, axis=0, keepdims=True)
        eb = e.astype(jnp.bfloat16)
        out = jnp.dot(vbuf[s, 0], eb[0:R], preferred_element_type=jnp.float32)
        for a in range(1, G):
            out += jnp.dot(
                vbuf[s, a], eb[a * R : (a + 1) * R], preferred_element_type=jnp.float32
            )
        pout = lax.dot_general(
            vp,
            pe.astype(jnp.bfloat16),
            (((0,), (0,)), ((), ())),
            preferred_element_type=jnp.float32,
        )
        if not first:
            shrink = jnp.exp2(mref[cq, j] - peak)
            pshrink = jnp.exp2(pmref[cq, j] - ppeak)
            total += lref[cq, j] * shrink
            ptotal += plref[cq, j] * pshrink
            out += acc[cq, j] * shrink
            pout += pacc[cq, j] * pshrink
        mref[cq, j] = peak
        lref[cq, j] = total
        acc[cq, j] = out
        pmref[cq, j] = ppeak
        plref[cq, j] = ptotal
        pacc[cq, j] = pout

    def back(i, n):
        src, dst = ((obox.at[n], abuf.at[c]), (lbox.at[n], lbuf.at[c]))[i]
        return pltpu.make_async_remote_copy(
            src_ref=src,
            dst_ref=dst,
            send_sem=back_send.at[i, n],
            recv_sem=back_recv.at[i, n],
            device_id=at(z, member(n + 1)),
            device_id_type=MESH,
        )

    def finish(n, who):
        for j in range(r):
            head = t * (G * r) + c * r + j
            gate_p = gbuf[who, pl.ds(head, 1), :]
            gate_s = gbuf[who, pl.ds(H + head, 1), :]
            total = lref[who, j]
            mixed_t = pacc[who, j] * (gate_p / plref[who, j]) + acc[who, j] * (gate_s / total)
            obox[n, :, j * HEAD_SIZE : (j + 1) * HEAD_SIZE] = mixed_t.T.astype(jnp.bfloat16)
            lbox[n, j : j + 1, :] = (mref[who, j] + jnp.log2(total)) * LN2

        @pl.when(n < G - 1)
        def _():
            back(0, n).start()
            back(1, n).start()

    def attend(s, first):
        def body(n, carry):
            who = lax.rem(c + 1 + n, G)
            for j in range(r):
                chunk(s, first, who, j)

            @pl.when(s == z)
            def _():
                finish(n, who)

            return carry

        late = G - early
        per = G // late
        for k in range(late):
            lax.fori_loop(k * per, (k + 1) * per if k < late - 1 else G, body, 0)
            pass_on(s + 1, early + k)

    attend(0, True)

    def step(s, carry):
        for g in range(early):
            pass_on(s + 1, g)
        attend(s, False)
        return carry

    lax.fori_loop(1, z + 1, step, 0)

    abuf[c] = obox[G - 1]
    lbuf[c] = lbox[G - 1]
    wo_copy.wait()
    for n in range(G - 1):
        back(0, n).wait_recv()
        back(1, n).wait_recv()
    for a in range(G):
        lse_out[a * r : (a + 1) * r, :] = lbuf[a, 0:r, :]

    piece = R // T

    def share(dest):
        rows = pl.ds(pl.multiple_of(dest * piece, piece), piece)
        total = None
        for a in range(G):
            term = jnp.dot(
                abuf[a, rows, :],
                wo[a * span : (a + 1) * span, :],
                preferred_element_type=jnp.float32,
            )
            total = term if total is None else total + term
        return total.astype(jnp.bfloat16)

    hops = []
    for o in range(1, T):
        dest = lax.rem(t + o, T)
        sbox[o] = share(dest)
        copy = pltpu.make_async_remote_copy(
            src_ref=sbox.at[o],
            dst_ref=rbox.at[o],
            send_sem=tp_send.at[o],
            recv_sem=tp_recv.at[o],
            device_id={"tp": dest},
            device_id_type=MESH,
        )
        copy.start()
        hops.append(copy)
    final = share(t).astype(jnp.float32)
    for o in range(1, T):
        hops[o - 1].wait_recv()
        final = final + rbox[o].astype(jnp.float32)
    mixed[...] = final.astype(jnp.bfloat16)

    for copy in hops:
        copy.wait_send()
    for g in range(1, G):
        for i in range(5):
            swap(i, g).wait_send()
        for i in range(2):
            back(i, g - 1).wait_send()

    @pl.when(z + 1 < Z)
    def _():
        def drain(s, carry):
            for g in range(G):
                for copy in chain(s, g):
                    copy.wait_send()
            return carry

        lax.fori_loop(0, z + 1, drain, 0)


def shards(
    tokens,
    query_weight,
    key_matrix,
    value_matrix,
    gate_weight,
    key_pool_weight,
    value_pool_weight,
    out_weight,
    chosen,
):
    R, width = tokens.shape
    kv_size = lax.axis_size("kv")
    T = lax.axis_size("tp")
    kv = lax.axis_index("kv")
    t = lax.axis_index("tp")
    G = key_matrix.shape[1] // HEAD_SIZE
    r = query_weight.shape[1] // key_matrix.shape[1]
    Z = kv_size // G
    H = gate_weight.shape[2]
    per_dev = chosen.shape[0]
    pooled = R // POOL_STRIDE
    nb = G * per_dev
    nbp = max(8, nb)
    span = r * HEAD_SIZE
    f32, bf16 = jnp.float32, jnp.bfloat16

    half = HEAD_SIZE // 2
    lane = jnp.arange(HEAD_SIZE, dtype=jnp.int32)
    inverse = THETA ** (-(lane % half).astype(f32) / half)
    positions = kv * R + jnp.arange(R, dtype=jnp.int32)
    angles = positions.astype(f32)[:, None] * inverse[None, :]
    cos = jnp.cos(angles)
    sin = jnp.sin(angles) * jnp.where(lane < half, -1.0, 1.0)[None, :]
    blocks = jnp.arange(kv_size * per_dev, dtype=jnp.int32)
    counts = jnp.sum((chosen[None] == blocks[:, None, None]).astype(f32), axis=2)
    counts = jnp.pad(counts.reshape(Z, nb, per_dev), ((0, 0), (0, nbp - nb), (0, 128 - per_dev)))

    vmem = pl.BlockSpec(memory_space=pltpu.VMEM)
    anywhere = pl.BlockSpec(memory_space=pl.ANY)
    sem = pltpu.SemaphoreType.DMA
    keys_shape = (R + 2 * pooled, HEAD_SIZE)
    out_width = out_weight.shape[1]
    mixed, lse = pl.pallas_call(
        functools.partial(attend_kernel, (G, Z, T, R, r, H)),
        in_specs=[anywhere] * 6 + [vmem] * 5,
        out_specs=[vmem, vmem],
        out_shape=[
            jax.ShapeDtypeStruct((R // T, out_width), bf16),
            jax.ShapeDtypeStruct((G * r, R), f32),
        ],
        scratch_shapes=[
            pltpu.VMEM((R, width), bf16),
            pltpu.VMEM((G, width, span), bf16),
            pltpu.VMEM((G, width, 2 * HEAD_SIZE), bf16),
            pltpu.VMEM(out_weight.shape, bf16),
            pltpu.VMEM((G, R, span), bf16),
            pltpu.VMEM((G, *keys_shape), bf16),
            pltpu.VMEM((G, HEAD_SIZE, R), bf16),
            pltpu.VMEM((2 * H, R), f32),
            pltpu.VMEM((G, R, span), bf16),
            pltpu.VMEM((Z, G, *keys_shape), bf16),
            pltpu.VMEM((Z, G, HEAD_SIZE, R), bf16),
            pltpu.VMEM((G, Z, nbp, 128), f32),
            pltpu.VMEM((G, 2 * H, R), f32),
            pltpu.VMEM((G, Z, nbp, R), f32),
            pltpu.VMEM((G, r, HEAD_SIZE, R), f32),
            pltpu.VMEM((G, r, 1, R), f32),
            pltpu.VMEM((G, r, 1, R), f32),
            pltpu.VMEM((G, r, HEAD_SIZE, R), f32),
            pltpu.VMEM((G, r, 1, R), f32),
            pltpu.VMEM((G, r, 1, R), f32),
            pltpu.VMEM((G, R, span), bf16),
            pltpu.VMEM((G, 8, R), f32),
            pltpu.VMEM((G, R, span), bf16),
            pltpu.VMEM((G, 8, R), f32),
            pltpu.VMEM((T, R // T, out_width), bf16),
            pltpu.VMEM((T, R // T, out_width), bf16),
            sem((3,)),
            sem((3, G)),
            sem((5, G)),
            sem((5, G)),
            sem((2, Z, G)),
            sem((2, Z, G)),
            sem((2, G)),
            sem((2, G)),
            sem((T,)),
            sem((T,)),
        ],
        compiler_params=pltpu.CompilerParams(collective_id=0, has_side_effects=True),
        name="attend",
    )(
        tokens,
        query_weight,
        key_matrix,
        value_matrix,
        out_weight,
        counts,
        jnp.swapaxes(gate_weight, 1, 2),
        key_pool_weight.T,
        value_pool_weight.T,
        cos,
        sin,
    )
    return mixed, lse.T


def solution(mesh):
    in_specs = (
        P("kv", None),
        P(None, "tp"),
        P(None, "tp"),
        P(None, "tp"),
        P(),
        P(),
        P(),
        P("tp", None),
        P("kv", None),
    )
    out_specs = (P(("kv", "tp"), None), P("kv", "tp"))
    return jax.shard_map(shards, mesh=mesh, in_specs=in_specs, out_specs=out_specs, check_vma=False)
```

time: 88.1 us -> 69.2 us (0.79)
  Pallas kernels: 77.4 us -> 61.8 us
  local copies, waits for them, and re-layouts: 8.36 us -> 3.89 us
    pallas_call x1 -> x0, Pallas kernels: 9.29 us -> none  [shards(): pl.pallas_call(functools.partial(project_kernel, r), grid=(G,), in_specs=...]
    pallas_call x1, Pallas kernels: 68.1 us -> 61.8 us  [shards(): pl.pallas_call(functools.partial(attend_kernel, (G, Z, T, R, r, H)), in_s...]
    slice x3 -> x0, local copies, waits for them, and re-layouts: 2.02 us -> none  [the longest x1 0.76 us: shards(): log_sums = lse[:, :r, :].reshape(G * r, R).T]
    unnamed x8 -> x2, local copies, waits for them, and re-layouts: 4.11 us -> 3.18 us
where the time goes in v2:
time: 69.2 us; the launch traced here: 68.4 us
  Pallas kernels  61.8 us (89%)
  local copies, waits for them, and re-layouts  3.89 us (6%)
  other arithmetic  2.03 us (3%)
    pallas_call x1, Pallas kernels, shards(): pl.pallas_call(functools.partial(attend_kernel, (G, Z, T, R, r, H)), in_s...  61.8 us
    unnamed x2, local copies, waits for them, and re-layouts  3.18 us

profile of v2, /device:TPU:25, one launch (start us, length us, event | category | flops | bytes accessed | tf_op | source)
XLA Modules:
  0.0 68.4 jit_solution(14022456536183715096)
XLA Ops:
  0.7 0.8 %convert_reduce_fusion = f32[64,4]{0,1:T(4,128)S(1)} fusion(s32[4,32]{1,0:T(4,128)} %param.17), kind=kLoop, calls=%fused_computation.3 | loop fusion | flops 24320 | bytes 1536 | tf_op jit(solution)/shard_map/reduce_sum | solution.py:474
  1.4 0.1 copy.11
  1.5 0.6 pad.4.cnt_in
  2.2 1.2 %fusion = (f32[256,128]{1,0:T(8,128)}, f32[256,128]{1,0:T(8,128)}) fusion(f32[128]{0:T(128)S(1)} %get-tuple-element.8, f32[128]{0:T(128)S(1)} %get-tuple-element.9, f32[256]{0:T(256)S(1)} %add_convert_fusion), kind=kLoop, calls=%fused_computation.2 | loop fusion | flops 65536 | bytes 264192 | tf_op jit(solution)/shard_map/mul | solution.py:472
  3.4 61.8 %attend.1 = (bf16[128,2048]{1,0:T(8,128)(2,1)}, f32[8,256]{1,0:T(8,128)}) custom-call(bf16[256,2048]{1,0:T(8,128)(2,1)} %x_in.1, bf16[2048,1024]{1,0:T(8,128)(2,1)} %wq_in.1, bf16[2048,512]{1,0:T(8,128)(2,1)} %wk_in.1, bf16[2048,512]{1,0:T(8,128)(2,1)} %wv_in.1, bf16[1024,2048]{1,0:T(8,128)(2,1)} %wo_in.1, f32[4,16,128]{2,1,0:T(8,128)} %pad.4.cnt_in, ...), custom_call_target="tpu_custom_call" | custom-call | tf_op jit(solution)/shard_map/attend/pallas_call | solution.py:482
  65.2 1.9 %copy.14 = bf16[128,2048]{1,0:T(8,128)(2,1)} copy(bf16[128,2048]{1,0:T(8,128)(2,1)} %get-tuple-element.12) | data formatting | bytes 1048576
  67.1 1.3 %copy.15 = f32[256,8]{0,1:T(8,128)} copy(f32[256,8]{0,1:T(8,128)} %bitcast.7) | data formatting | bytes 16384
  (2 shorter events, 0.0 us)
